TPU v7x, 32 devices: a whole 2x2x4 slice. The times are simulated.
32 devices in a mesh: sp: 4 (over z), dp: 8 (over y, x, core).
Axes of the slice: x: 2, y: 2, z: 4, core: 2. Of those that a mesh axis runs over, the one named last changes fastest.
Arguments:
- hidden: bfloat16 [8, 512, 2048], P('dp', 'sp'), may hold values from -6 to 6
- queries: bfloat16 [8, 512, 1024], P('dp', 'sp'), may hold values from -6 to 6
- values: bfloat16 [8, 512, 2048], P('dp', 'sp'), may hold values from -6 to 6
- key_weight: bfloat16 [2048, 1024], P('dp'), may hold values from -0.125 to 0.125
- decay_down: bfloat16 [2048, 16], replicated, may hold values from -0.125 to 0.125
- decay_up: float32 [16, 1024], replicated, may hold values from -1.5 to 1.5
- decay_bias: float32 [1024], replicated, may hold values from -1 to 8
- span_shift: bfloat16 [8, 512], P('dp', 'sp'), may hold values from -1.5 to 1.5, as said below
- norm_gain: float32 [2048], replicated, may hold values from 0.1 to 1.9
Outputs:
- attended: bfloat16 [8, 512, 2048], P('dp', 'sp')
Inputs may be any that keep to these rules, and one draw needn't show every extreme that they name: `span_shift`: constant over each aligned block of 64 positions.
All inputs are finite; a program needn't handle non-finite values.
Results may differ from a plain program's by a relative error of at most 0.0073.
Values may be sent and summed in bfloat16 or wider, within the bound.
A program may use at most 64 MiB of HBM per device.

v0:
```python
import jax
import jax.numpy as jnp
from jax import lax
from jax.sharding import PartitionSpec as P

HEADS = 4
DK = 256
DV = 512
BLOCK = 64
KEY = 1024
VAL = 2048
decay_tau = 16.0
norm_eps = 1e-05
highest = lax.Precision.HIGHEST


def mechanism(query, keys_in, value_in, log_decay):
    length, key_width = query.shape
    value_width = value_in.shape[-1]
    blocks = length // BLOCK
    step_decay = log_decay.reshape(blocks, BLOCK, key_width)
    inclusive = jnp.cumsum(step_decay, axis=1)
    exclusive = inclusive - step_decay
    total = inclusive[:, -1, :]
    query3 = query.reshape(blocks, BLOCK, key_width)
    keys3 = keys_in.reshape(blocks, BLOCK, key_width)
    value_tensor3 = value_in.reshape(blocks, BLOCK, value_width)
    query_forward_part = (query3 * jnp.exp(inclusive)).astype(jnp.bfloat16)
    key_fwd = (keys3 * jnp.exp(-inclusive)).astype(jnp.bfloat16)
    query_reverse_part = (query3 * jnp.exp(-exclusive)).astype(jnp.bfloat16)
    key_bwd = (keys3 * jnp.exp(exclusive)).astype(jnp.bfloat16)
    key_end = (keys3 * jnp.exp(total[:, None, :] - inclusive)).astype(jnp.bfloat16)
    fwd_scores = jnp.einsum(
        "nid,njd->nij", query_forward_part, key_fwd, preferred_element_type=jnp.float32
    )
    bwd_scores = jnp.einsum(
        "nid,njd->nij", query_reverse_part, key_bwd, preferred_element_type=jnp.float32
    )
    row_index = lax.broadcasted_iota(jnp.int32, (BLOCK, BLOCK), 0)
    col_index = lax.broadcasted_iota(jnp.int32, (BLOCK, BLOCK), 1)
    attention_scores = jnp.where((col_index <= row_index)[None], fwd_scores, bwd_scores).astype(
        jnp.bfloat16
    )
    inner_block_term = jnp.einsum(
        "ucy,uyh->uch", attention_scores, value_tensor3, preferred_element_type=jnp.float32
    )
    end_terms = jnp.einsum(
        "njd,nje->nde", key_end, value_tensor3, preferred_element_type=jnp.float32
    )
    start_terms = jnp.einsum(
        "njd,nje->nde", key_bwd, value_tensor3, preferred_element_type=jnp.float32
    )
    rates = jnp.exp(total)

    def forward_step(carry_state, inputs):
        rate, term = inputs
        return (rate[:, None] * carry_state + term, carry_state)

    def backward_step(carry_state, inputs):
        rate, term = inputs
        state_here = rate[:, None] * carry_state
        return (state_here + term, state_here)

    empty = jnp.zeros((key_width, value_width), jnp.float32)
    _, forward_scan_states = lax.scan(forward_step, empty, (rates, end_terms))
    _, reverse_scan_states = lax.scan(backward_step, empty, (rates, start_terms), reverse=True)
    produced_rows = jnp.einsum(
        "tzv,tvg->tzg",
        query_forward_part,
        forward_scan_states.astype(jnp.bfloat16),
        preferred_element_type=jnp.float32,
    )
    produced_rows = produced_rows + jnp.einsum(
        "tzv,tvg->tzg",
        query_reverse_part,
        reverse_scan_states.astype(jnp.bfloat16),
        preferred_element_type=jnp.float32,
    )
    return (inner_block_term + produced_rows).reshape(length, value_width).astype(jnp.bfloat16)


def body(
    hidden, queries, values, key_weight, decay_down, decay_up, decay_bias, span_shift, norm_gain
):
    seq_count, tok_count, model_width = hidden.shape
    group_size = lax.axis_size("sp")
    value_split = group_size // HEADS
    part_width = DV // value_split
    head_index = lax.axis_index("sp") // value_split
    token_rows = hidden.reshape(tok_count, model_width)

    def per_item(tensor, width):
        by_head = tensor.reshape(tok_count, HEADS, width).transpose(1, 0, 2)
        spread_out = jnp.broadcast_to(by_head[:, None], (HEADS, value_split, tok_count, width))
        return spread_out.reshape(group_size, tok_count, width)

    def every_item(tensor):
        return jnp.broadcast_to(tensor[None], (group_size,) + tensor.shape)

    key_sums = jnp.dot(
        token_rows,
        lax.all_gather(key_weight, "dp", axis=0, tiled=True),
        preferred_element_type=jnp.float32,
    )
    keys = key_sums.astype(jnp.bfloat16)
    head_key = lax.all_to_all(per_item(keys, DK), "sp", split_axis=0, concat_axis=1, tiled=True)[0]
    low = jnp.dot(token_rows, decay_down, preferred_element_type=jnp.float32).astype(jnp.bfloat16)
    value_items = values.reshape(tok_count, group_size, part_width).transpose(1, 0, 2)
    head_query, head_value, head_low, head_shift = (
        lax.all_to_all(
            per_item(queries.reshape(tok_count, KEY), DK),
            "sp",
            split_axis=0,
            concat_axis=1,
            tiled=True,
        ),
        lax.all_to_all(value_items, "sp", split_axis=0, concat_axis=1, tiled=True),
        lax.all_to_all(every_item(low), "sp", split_axis=0, concat_axis=1, tiled=True),
        lax.all_to_all(
            every_item(span_shift.reshape(tok_count, 1)),
            "sp",
            split_axis=0,
            concat_axis=1,
            tiled=True,
        ),
    )
    up_columns = lax.dynamic_slice_in_dim(decay_up, head_index * DK, DK, 1)
    bias_part = lax.dynamic_slice_in_dim(decay_bias, head_index * DK, DK, 0)
    pre = jnp.dot(
        head_low[0].astype(jnp.float32),
        up_columns,
        precision=highest,
        preferred_element_type=jnp.float32,
    )
    pre = pre + bias_part[None, :] + head_shift[0].astype(jnp.float32)
    log_decay = jax.nn.log_sigmoid(pre) / decay_tau
    scaled = head_query[0].astype(jnp.float32) * DK ** (-0.5)
    mixed = mechanism(scaled, head_key.astype(jnp.float32), head_value[0], log_decay)
    returned = lax.all_to_all(mixed[None], "sp", split_axis=1, concat_axis=0, tiled=True)
    grouped = returned.astype(jnp.float32).transpose(1, 0, 2).reshape(tok_count, HEADS, DV)
    normed = grouped * lax.rsqrt(jnp.mean(grouped * grouped, axis=-1, keepdims=True) + norm_eps)
    normed = normed * norm_gain.reshape(HEADS, DV)[None]
    return normed.reshape(seq_count, tok_count, VAL).astype(jnp.bfloat16)


def solution(mesh):
    in_specs = (
        P("dp", "sp", None),
        P("dp", "sp", None),
        P("dp", "sp", None),
        P("dp", None),
        P(),
        P(),
        P(),
        P("dp", "sp"),
        P(),
    )
    out_specs = P("dp", "sp", None)
    return jax.shard_map(body, mesh=mesh, in_specs=in_specs, out_specs=out_specs, check_vma=False)
```

profile of v0, /device:TPU:0, one launch (start us, length us, event | category | flops | bytes accessed | tf_op | source)
XLA Modules:
  0.0 159.2 jit_solution(2826352887242074970)
XLA Ops:
  7.3 1.2 broadcast_in_dim.46
  8.5 6.3 %all-to-all-start.2 = ((bf16[4,128,1]{1,2,0:T(2,128)(2,1)}), bf16[4,128,1]{1,2,0:T(2,128)(2,1)S(1)}, u32[]{:S(2)}, u32[]{:S(2)}) async-start(bf16[4,128,1]{1,2,0:T(2,128)(2,1)} %broadcast_in_dim.46), calls=%async_computation.2 | async-start | bytes 4096 | tf_op jit(solution)/shard_map/all_to_all | solution.py:119
  14.8 1.1 convolution_convert_fusion.1
  15.9 4.4 %all-to-all-done.2 = bf16[4,128,1]{1,2,0:T(2,128)(2,1)S(1)} async-done(((bf16[4,128,1]{1,2,0:T(2,128)(2,1)}), bf16[4,128,1]{1,2,0:T(2,128)(2,1)S(1)}, u32[]{:S(2)}, u32[]{:S(2)}) %all-to-all-start.2) | async-done | bytes 1056 | tf_op jit(solution)/shard_map/all_to_all | solution.py:119
  21.0 3.3 %all-to-all-start.1 = ((bf16[4,128,16]{1,2,0:T(8,128)(2,1)}), bf16[4,128,16]{1,2,0:T(8,128)(2,1)S(1)}, u32[]{:S(2)}, u32[]{:S(2)}) async-start(bf16[4,128,16]{1,2,0:T(8,128)(2,1)} %broadcast_in_dim.44), calls=%async_computation.1 | async-start | bytes 32768 | tf_op jit(solution)/shard_map/all_to_all | solution.py:118
  24.2 1.8 %copy.72 = bf16[1,128,1024]{1,2,0:T(8,128)(2,1)} copy(bf16[1,128,1024]{2,1,0:T(8,128)(2,1)} %param.14) | data formatting | bytes 524288 | tf_op args[1]
  26.0 3.8 %all-to-all-done.1 = bf16[4,128,16]{1,2,0:T(8,128)(2,1)S(1)} async-done(((bf16[4,128,16]{1,2,0:T(8,128)(2,1)}), bf16[4,128,16]{1,2,0:T(8,128)(2,1)S(1)}, u32[]{:S(2)}, u32[]{:S(2)}) %all-to-all-start.1) | async-done | bytes 16416 | tf_op jit(solution)/shard_map/all_to_all | solution.py:118
  29.8 3.4 %all-to-all-start = ((bf16[4,128,256]{1,2,0:T(8,128)(2,1)}), bf16[4,128,256]{1,2,0:T(8,128)(2,1)S(1)}, u32[]{:S(2)}, u32[]{:S(2)}) async-start(bf16[4,128,256]{1,2,0:T(8,128)(2,1)} %bitcast.1), calls=%async_computation | async-start | bytes 524288 | tf_op jit(solution)/shard_map/all_to_all | solution.py:110
  33.6 0.9 copy.134
  34.5 0.8 dynamic_slice.33
  35.3 13.3 %all-gather.2.cloned.1.call-done = bf16[2048,1024]{1,0:T(8,128)(2,1)} async-done(((bf16[256,1024]{1,0:T(8,128)(2,1)}), bf16[2048,1024]{1,0:T(8,128)(2,1)}) %all-gather.2.cloned.1.call-update) | async-done | bytes 4194320 | tf_op jit(solution)/shard_map/all_gather | solution.py:102
  48.6 2.9 %convolution_convert_fusion = bf16[128,1024]{1,0:T(8,128)(2,1)S(1)} fusion(bf16[2048,1024]{1,0:T(8,128)(2,1)} %all-gather.2.cloned.1.call-done, bf16[1,128,2048]{2,1,0:T(8,128)(2,1)S(1)} %copy-done), kind=kOutput, calls=%fused_computation.18 | convolution fusion | flops 537001984 | bytes 4980736 | tf_op jit(solution)/shard_map/dot_general | solution.py:100
  52.2 4.6 %all-to-all-start.3 = ((bf16[4,128,256]{2,1,0:T(8,128)(2,1)}), bf16[4,128,256]{2,1,0:T(8,128)(2,1)S(1)}, u32[]{:S(2)}, u32[]{:S(2)}) async-start(bf16[4,128,256]{2,1,0:T(8,128)(2,1)} %bitcast.59), calls=%async_computation.3 | async-start | bytes 524288 | tf_op jit(solution)/shard_map/all_to_all | solution.py:106
  56.8 1.4 fusion.12
  58.2 0.8 copy-done.2
  59.3 6.8 %all-to-all-done.3 = bf16[4,128,256]{2,1,0:T(8,128)(2,1)S(1)} async-done(((bf16[4,128,256]{2,1,0:T(8,128)(2,1)}), bf16[4,128,256]{2,1,0:T(8,128)(2,1)S(1)}, u32[]{:S(2)}, u32[]{:S(2)}) %all-to-all-start.3) | async-done | bytes 262176 | tf_op jit(solution)/shard_map/all_to_all | solution.py:106
  66.8 3.7 %all-to-all-start.4 = ((bf16[4,128,512]{2,1,0:T(8,128)(2,1)}), bf16[4,128,512]{2,1,0:T(8,128)(2,1)S(1)}, u32[]{:S(2)}, u32[]{:S(2)}) async-start(bf16[4,128,512]{2,1,0:T(8,128)(2,1)} %bitcast.57), calls=%async_computation.4 | async-start | bytes 1048576 | tf_op jit(solution)/shard_map/all_to_all | solution.py:117
  70.6 1.0 copy.73
  71.6 1.0 convert.4
  72.6 3.1 %multiply_convert_fusion.4 = (bf16[8,64,256]{2,0,1:T(8,128)(2,1)}, bf16[8,64,256]{2,0,1:T(8,128)(2,1)S(1)}, bf16[8,64,256]{2,0,1:T(8,128)(2,1)S(1)}, bf16[8,64,256]{2,0,1:T(8,128)(2,1)S(1)}, bf16[8,64,256]{2,0,1:T(8,128)(2,1)}) fusion(f32[8,64,256]{2,0,1:T(8,128)S(1)} %fusion.15, f32[8,64,256]{2,1,0:T(8,128)S(1)} %convert.4, f32[8,64,256]{2,1,0:T(8,128)} %bitcast.82, ...), kind=kLoop, calls=%fused_computation.32 | loop fusion | flops 1835008 | bytes 3416064 | tf_op jit(solution)/shard_map/convert_element_type | solution.py:29
  75.7 7.6 %all-to-all-done.4 = bf16[4,128,512]{2,1,0:T(8,128)(2,1)S(1)} async-done(((bf16[4,128,512]{2,1,0:T(8,128)(2,1)}), bf16[4,128,512]{2,1,0:T(8,128)(2,1)S(1)}, u32[]{:S(2)}, u32[]{:S(2)}) %all-to-all-start.4) | async-done | bytes 524320 | tf_op jit(solution)/shard_map/all_to_all | solution.py:117
  83.3 2.7 %fusion.21 = f32[8,256,512]{2,1,0:T(8,128)} fusion(bf16[8,64,512]{2,1,0:T(8,128)(2,1)S(1)} %bitcast.75, bf16[8,64,256]{2,0,1:T(8,128)(2,1)S(1)} %get-tuple-element.194), kind=kOutput, calls=%fused_computation.43 | convolution fusion | flops 134217728 | bytes 4980736 | tf_op jit(solution)/shard_map/njd,nje->nde/dot_general | solution.py:50
  86.0 1.5 broadcast.22.clone
  87.6 16.1 %while.31 = (s32[]{:T(128)}, f32[256,512]{1,0:T(8,128)S(1)}, bf16[8,256,512]{2,1,0:T(8,128)(2,1)}, f32[8,256]{1,0:T(8,128)S(1)}, f32[8,256,512]{2,1,0:T(8,128)}, /*index=5*/s32[]{:T(128)}, s32[]{:T(128)}, s32[]{:T(128)}) while((s32[]{:T(128)}, f32[256,512]{1,0:T(8,128)S(1)}, bf16[8,256,512]{2,1,0:T(8,128)(2,1)}, ...), condition=%wide.region_4.5_spmd.clone, body=%wide.region_3.4_spmd.clone.sunk | while | flops 655364 | bytes 2625656 | solution.py:66
  87.6 0.8 bitcast_dynamic-update-slice_fusion.5
  88.4 1.2 bitcast_add_fusion.5
  89.6 0.8 bitcast_dynamic-update-slice_fusion.5
  90.4 1.2 bitcast_add_fusion.5
  91.6 0.8 bitcast_dynamic-update-slice_fusion.5
  92.4 1.2 bitcast_add_fusion.5
  93.6 0.8 bitcast_dynamic-update-slice_fusion.5
  94.5 1.2 bitcast_add_fusion.5
  95.6 0.8 bitcast_dynamic-update-slice_fusion.5
  96.5 1.2 bitcast_add_fusion.5
  97.7 0.8 bitcast_dynamic-update-slice_fusion.5
  98.5 1.2 bitcast_add_fusion.5
  99.7 0.8 bitcast_dynamic-update-slice_fusion.5
  100.5 1.2 bitcast_add_fusion.5
  101.7 0.8 bitcast_dynamic-update-slice_fusion.5
  102.5 1.2 bitcast_add_fusion.5
  103.7 2.7 %fusion.17 = f32[8,256,512]{2,1,0:T(8,128)} fusion(bf16[8,64,512]{2,1,0:T(8,128)(2,1)S(1)} %bitcast.76, bf16[8,64,256]{2,0,1:T(8,128)(2,1)S(1)} %copy-done.4), kind=kOutput, calls=%fused_computation.39 | convolution fusion | flops 134217728 | bytes 4980736 | tf_op jit(solution)/shard_map/njd,nje->nde/dot_general | solution.py:47
  106.4 1.5 broadcast.22.clone.1
  107.9 15.5 %while.30 = (s32[]{:T(128)}, f32[256,512]{1,0:T(8,128)S(1)}, bf16[8,256,512]{2,1,0:T(8,128)(2,1)}, f32[8,256]{1,0:T(8,128)S(1)}, f32[8,256,512]{2,1,0:T(8,128)}, /*index=5*/s32[]{:T(128)}, s32[]{:T(128)}) while((s32[]{:T(128)}, f32[256,512]{1,0:T(8,128)S(1)}, bf16[8,256,512]{2,1,0:T(8,128)(2,1)}, f32[8,256]{1,0:T(8,128)S(1)}, ...), condition=%wide.region_2.3_spmd.clone, body=%wide.region_1.2_spmd.clone.sunk | while | flops 524291 | bytes 2362976 | solution.py:65
  107.9 0.7 bitcast_dynamic-update-slice_fusion.4
  108.7 1.2 bitcast_add_fusion.4
  109.8 0.8 bitcast_dynamic-update-slice_fusion.4
  110.6 1.2 bitcast_add_fusion.4
  111.8 0.8 bitcast_dynamic-update-slice_fusion.4
  112.6 1.2 bitcast_add_fusion.4
  114.5 1.2 bitcast_add_fusion.4
  116.4 1.2 bitcast_add_fusion.4
  117.6 0.7 bitcast_dynamic-update-slice_fusion.4
  118.3 1.2 bitcast_add_fusion.4
  119.5 0.8 bitcast_dynamic-update-slice_fusion.4
  120.3 1.2 bitcast_add_fusion.4
  121.4 0.8 bitcast_dynamic-update-slice_fusion.4
  122.2 1.2 bitcast_add_fusion.4
  123.4 2.2 %fusion = f32[8,64,512]{2,1,0:T(8,128)S(1)} fusion(bf16[8,256,512]{2,1,0:T(8,128)(2,1)} %get-tuple-element.136, bf16[8,64,256]{2,0,1:T(8,128)(2,1)S(1)} %get-tuple-element.195), kind=kOutput, calls=%fused_computation.7 | convolution fusion | flops 134217728 | bytes 3407872 | tf_op jit(solution)/shard_map/tzv,tvg->tzg/dot_general | solution.py:73
  126.7 0.8 copy.136
  128.1 3.8 %reduce = bf16[512,512]{1,0:T(8,128)(2,1)S(1)} reduce(bf16[512,1,512]{2,1,0:T(2,128)(2,1)S(1)} %bitcast.78, bf16[]{:T(256)} %broadcast.39), dimensions={1}, to_apply=%bitcast.60.reduce_sub_computation | reduce | bytes 1048578
  131.9 1.2 reshape.113
  133.1 3.5 %all-to-all-start.5 = ((bf16[4,2,32768]{2,1,0:T(2,128)(2,1)}), bf16[4,2,32768]{2,1,0:T(2,128)(2,1)S(1)}, u32[]{:S(2)}, u32[]{:S(2)}) async-start(bf16[4,2,32768]{2,1,0:T(2,128)(2,1)} %reshape.113), calls=%async_computation.5 | async-start | bytes 1048576 | tf_op jit(solution)/shard_map/all_to_all | solution.py:139
  136.6 13.2 %all-to-all-done.5 = bf16[4,2,32768]{2,1,0:T(2,128)(2,1)S(1)} async-done(((bf16[4,2,32768]{2,1,0:T(2,128)(2,1)}), bf16[4,2,32768]{2,1,0:T(2,128)(2,1)S(1)}, u32[]{:S(2)}, u32[]{:S(2)}) %all-to-all-start.5) | async-done | bytes 524320 | tf_op jit(solution)/shard_map/all_to_all | solution.py:139
  151.2 1.2 convert_element_type.104
  (58 shorter events, 8.1 us)
Async XLA Ops:
  6.5 8.3 %copy-start = (bf16[1,128,2048]{2,1,0:T(8,128)(2,1)S(1)}, bf16[1,128,2048]{2,1,0:T(8,128)(2,1)}, u32[]{:S(2)}) copy-start(bf16[1,128,2048]{2,1,0:T(8,128)(2,1)} %param.13) | copy-start | bytes 1572868
  6.5 26.7 %copy-start.5 = (bf16[1,128,2048]{2,1,0:T(8,128)(2,1)S(1)}, bf16[1,128,2048]{2,1,0:T(8,128)(2,1)}, u32[]{:S(2)}) copy-start(bf16[1,128,2048]{2,1,0:T(8,128)(2,1)} %param.15) | copy-start | bytes 1572868
  6.5 42.0 %all-gather.2.cloned.1.call-start = ((), (), s32[]{:S(2)}) async-start(), calls=%async_computation.6 | async-start | bytes 4718592 | tf_op jit(solution)/shard_map/all_gather | solution.py:102
  8.5 11.8 %all-to-all-start.2 = ((bf16[4,128,1]{1,2,0:T(2,128)(2,1)}), bf16[4,128,1]{1,2,0:T(2,128)(2,1)S(1)}, u32[]{:S(2)}, u32[]{:S(2)}) async-start(bf16[4,128,1]{1,2,0:T(2,128)(2,1)} %broadcast_in_dim.46), calls=%async_computation.2 | async-start | bytes 4096 | tf_op jit(solution)/shard_map/all_to_all | solution.py:119
  21.0 8.8 %all-to-all-start.1 = ((bf16[4,128,16]{1,2,0:T(8,128)(2,1)}), bf16[4,128,16]{1,2,0:T(8,128)(2,1)S(1)}, u32[]{:S(2)}, u32[]{:S(2)}) async-start(bf16[4,128,16]{1,2,0:T(8,128)(2,1)} %broadcast_in_dim.44), calls=%async_computation.1 | async-start | bytes 32768 | tf_op jit(solution)/shard_map/all_to_all | solution.py:118
  29.8 22.4 %all-to-all-start = ((bf16[4,128,256]{1,2,0:T(8,128)(2,1)}), bf16[4,128,256]{1,2,0:T(8,128)(2,1)S(1)}, u32[]{:S(2)}, u32[]{:S(2)}) async-start(bf16[4,128,256]{1,2,0:T(8,128)(2,1)} %bitcast.1), calls=%async_computation | async-start | bytes 524288 | tf_op jit(solution)/shard_map/all_to_all | solution.py:110
  52.2 13.9 %all-to-all-start.3 = ((bf16[4,128,256]{2,1,0:T(8,128)(2,1)}), bf16[4,128,256]{2,1,0:T(8,128)(2,1)S(1)}, u32[]{:S(2)}, u32[]{:S(2)}) async-start(bf16[4,128,256]{2,1,0:T(8,128)(2,1)} %bitcast.59), calls=%async_computation.3 | async-start | bytes 524288 | tf_op jit(solution)/shard_map/all_to_all | solution.py:106
  58.2 0.8 copy-start.2
  66.1 0.7 copy-start.3
  66.8 16.5 %all-to-all-start.4 = ((bf16[4,128,512]{2,1,0:T(8,128)(2,1)}), bf16[4,128,512]{2,1,0:T(8,128)(2,1)S(1)}, u32[]{:S(2)}, u32[]{:S(2)}) async-start(bf16[4,128,512]{2,1,0:T(8,128)(2,1)} %bitcast.57), calls=%async_computation.4 | async-start | bytes 1048576 | tf_op jit(solution)/shard_map/all_to_all | solution.py:117
  87.6 16.1 %copy-start.4 = (bf16[8,64,256]{2,0,1:T(8,128)(2,1)S(1)}, bf16[8,64,256]{2,0,1:T(8,128)(2,1)}, u32[]{:S(2)}) copy-start(bf16[8,64,256]{2,0,1:T(8,128)(2,1)} %get-tuple-element.197) | copy-start | bytes 786436
  123.4 2.2 %copy-start.6 = (bf16[8,64,256]{2,0,1:T(8,128)(2,1)S(1)}, bf16[8,64,256]{2,0,1:T(8,128)(2,1)}, u32[]{:S(2)}) copy-start(bf16[8,64,256]{2,0,1:T(8,128)(2,1)} %get-tuple-element.193) | copy-start | bytes 786436
  123.4 2.4 %copy-start.1 = (bf16[8,256,512]{2,1,0:T(8,128)(2,1)S(1)}, bf16[8,256,512]{2,1,0:T(8,128)(2,1)}, u32[]{:S(2)}) copy-start(bf16[8,256,512]{2,1,0:T(8,128)(2,1)} %get-tuple-element.135) | copy-start | bytes 6291460
  127.5 9.0 %copy-start.7 = (f32[2048]{0:T(1024)S(1)}, f32[2048]{0:T(1024)}, u32[]{:S(2)}) copy-start(f32[2048]{0:T(1024)} %param.21) | copy-start | bytes 24580
  133.1 16.7 %all-to-all-start.5 = ((bf16[4,2,32768]{2,1,0:T(2,128)(2,1)}), bf16[4,2,32768]{2,1,0:T(2,128)(2,1)S(1)}, u32[]{:S(2)}, u32[]{:S(2)}) async-start(bf16[4,2,32768]{2,1,0:T(2,128)(2,1)} %reshape.113), calls=%async_computation.5 | async-start | bytes 1048576 | tf_op jit(solution)/shard_map/all_to_all | solution.py:139
Sparse Core Ops, SparseCore 0:
  9.2 39.2 all-gather.1
where the time goes:
time: 161 us; the launch traced here: 159 us
  waiting for transfers between devices  49.8 us (31%)
  other arithmetic  39.6 us (25%)
  starting transfers between devices  24.7 us (15%)
  local copies, waits for them, and re-layouts  16.8 us (10%)
  matrix products  14.1 us (9%)
  between operations  13.7 us (9%)
    all_gather x1, waiting for transfers between devices, body(): lax.all_gather(key_weight, 'dp', axis=0, tiled=True)  13.3 us
    all_to_all x1, waiting for transfers between devices, body(): lax.all_to_all(mixed[None], 'sp', split_axis=1, concat_axis=0, tiled=True)  13.2 us
    dynamic_update_slice x16, other arithmetic, mechanism(): _, forward_scan_states = lax.scan(forward_step, empty, (rates, end_terms))  12.6 us
    add x8, other arithmetic, forward_step(): return (rate[:, None] * carry_state + term, carry_state)  9.24 us
    add x8, other arithmetic, backward_step(): return (state_here + term, state_here)  9.24 us
    all_to_all x1, waiting for transfers between devices, body(): lax.all_to_all(value_items, 'sp', split_axis=0, concat_axis=1, tiled=True)  7.64 us
    all_to_all x1, waiting for transfers between devices, body(): lax.all_to_all(per_item(keys, DK), 'sp', split_axis=0, concat_axis=1, til...  6.78 us
    all_to_all x1, starting transfers between devices, body(): lax.all_to_all(every_item(span_shift.reshape(tok_count, 1)), 'sp', split_...  6.35 us
  transfers between devices with their start and end apart: 7, of which 6 were waited for; matrix products, arithmetic and copies ran while one was open for 11% of the time, Pallas kernels for 0%

commit v1 on v0

--- a/solution.py
+++ b/solution.py
@@ -1,3 +1,4 @@
+import functools
 import jax
 import jax.numpy as jnp
 from jax import lax
@@ -12,6 +13,17 @@
 decay_tau = 16.0
 norm_eps = 1e-05
 highest = lax.Precision.HIGHEST
+
+
+def _recast_slot(row_data, axis_id):
+    f_next = lax.all_to_all(
+        jnp.stack(jnp.split(row_data, lax.axis_size(axis_id), axis=1)), axis_id, 0, 0
+    )
+    right_arr = jnp.concatenate(f_next, axis=0)
+    return right_arr
+
+
+use_bench = functools.partial(_recast_slot, axis_id="sp")
 
 
 def mechanism(query, keys_in, value_in, log_decay):
@@ -136,7 +148,7 @@
     log_decay = jax.nn.log_sigmoid(pre) / decay_tau
     scaled = head_query[0].astype(jnp.float32) * DK ** (-0.5)
     mixed = mechanism(scaled, head_key.astype(jnp.float32), head_value[0], log_decay)
-    returned = lax.all_to_all(mixed[None], "sp", split_axis=1, concat_axis=0, tiled=True)
+    returned = use_bench(mixed[None])
     grouped = returned.astype(jnp.float32).transpose(1, 0, 2).reshape(tok_count, HEADS, DV)
     normed = grouped * lax.rsqrt(jnp.mean(grouped * grouped, axis=-1, keepdims=True) + norm_eps)
     normed = normed * norm_gain.reshape(HEADS, DV)[None]

time: 161 us -> 154 us (0.957)
  local copies, waits for them, and re-layouts: 16.8 us -> 12.2 us
  other arithmetic: 39.6 us -> 36.7 us
    unnamed x3 -> x2, other arithmetic: 3.82 us -> 0.01 us
    unnamed x21 -> x17, local copies, waits for them, and re-layouts: 5.61 us -> 1.85 us
where the time goes in v1:
time: 154 us; the launch traced here: 152 us
  waiting for transfers between devices  50.8 us (33%)
  other arithmetic  36.7 us (24%)
  starting transfers between devices  24.6 us (16%)
  matrix products  14.1 us (9%)
  between operations  13.7 us (9%)
  local copies, waits for them, and re-layouts  12.2 us (8%)
    all_gather x1, waiting for transfers between devices, body(): lax.all_gather(key_weight, 'dp', axis=0, tiled=True)  13.3 us
    all_to_all x1, waiting for transfers between devices, _recast_slot(): lax.all_to_all(jnp.stack(jnp.split(row_data, lax.axis_size(axis_id), axis...  13.2 us
    dynamic_update_slice x16, other arithmetic, mechanism(): _, forward_scan_states = lax.scan(forward_step, empty, (rates, end_terms))  12.5 us
    add x8, other arithmetic, backward_step(): return (state_here + term, state_here)  9.24 us
    add x8, other arithmetic, forward_step(): return (rate[:, None] * carry_state + term, carry_state)  9.24 us
    all_to_all x1, waiting for transfers between devices, body(): lax.all_to_all(value_items, 'sp', split_axis=0, concat_axis=1, tiled=True)  7.86 us
    all_to_all x1, waiting for transfers between devices, body(): lax.all_to_all(per_item(keys, DK), 'sp', split_axis=0, concat_axis=1, til...  7.53 us
    all_to_all x1, starting transfers between devices, body(): lax.all_to_all(every_item(span_shift.reshape(tok_count, 1)), 'sp', split_...  6.35 us
  transfers between devices with their start and end apart: 7, of which 6 were waited for; matrix products, arithmetic and copies ran while one was open for 11% of the time, Pallas kernels for 0%

profile of v1, /device:TPU:0, one launch (start us, length us, event | category | flops | bytes accessed | tf_op | source)
XLA Modules:
  0.0 152.4 jit_solution(9707913491749973782)
XLA Ops:
  7.3 1.2 broadcast_in_dim.46
  8.5 6.3 %all-to-all-start.2 = ((bf16[4,128,1]{1,2,0:T(2,128)(2,1)}), bf16[4,128,1]{1,2,0:T(2,128)(2,1)S(1)}, u32[]{:S(2)}, u32[]{:S(2)}) async-start(bf16[4,128,1]{1,2,0:T(2,128)(2,1)} %broadcast_in_dim.46), calls=%async_computation.2 | async-start | bytes 4096 | tf_op jit(solution)/shard_map/all_to_all | solution.py:131
  14.8 1.1 convolution_convert_fusion.1
  15.9 4.4 %all-to-all-done.2 = bf16[4,128,1]{1,2,0:T(2,128)(2,1)S(1)} async-done(((bf16[4,128,1]{1,2,0:T(2,128)(2,1)}), bf16[4,128,1]{1,2,0:T(2,128)(2,1)S(1)}, u32[]{:S(2)}, u32[]{:S(2)}) %all-to-all-start.2) | async-done | bytes 1056 | tf_op jit(solution)/shard_map/all_to_all | solution.py:131
  21.0 3.3 %all-to-all-start.1 = ((bf16[4,128,16]{1,2,0:T(8,128)(2,1)}), bf16[4,128,16]{1,2,0:T(8,128)(2,1)S(1)}, u32[]{:S(2)}, u32[]{:S(2)}) async-start(bf16[4,128,16]{1,2,0:T(8,128)(2,1)} %broadcast_in_dim.44), calls=%async_computation.1 | async-start | bytes 32768 | tf_op jit(solution)/shard_map/all_to_all | solution.py:130
  24.2 1.8 %copy.71 = bf16[1,128,1024]{1,2,0:T(8,128)(2,1)} copy(bf16[1,128,1024]{2,1,0:T(8,128)(2,1)} %param.14) | data formatting | bytes 524288 | tf_op args[1]
  26.0 3.8 %all-to-all-done.1 = bf16[4,128,16]{1,2,0:T(8,128)(2,1)S(1)} async-done(((bf16[4,128,16]{1,2,0:T(8,128)(2,1)}), bf16[4,128,16]{1,2,0:T(8,128)(2,1)S(1)}, u32[]{:S(2)}, u32[]{:S(2)}) %all-to-all-start.1) | async-done | bytes 16416 | tf_op jit(solution)/shard_map/all_to_all | solution.py:130
  29.8 3.4 %all-to-all-start = ((bf16[4,128,256]{1,2,0:T(8,128)(2,1)}), bf16[4,128,256]{1,2,0:T(8,128)(2,1)S(1)}, u32[]{:S(2)}, u32[]{:S(2)}) async-start(bf16[4,128,256]{1,2,0:T(8,128)(2,1)} %bitcast.1), calls=%async_computation | async-start | bytes 524288 | tf_op jit(solution)/shard_map/all_to_all | solution.py:122
  33.6 0.9 copy.130
  34.5 0.8 dynamic_slice.33
  35.3 13.3 %all-gather.2.cloned.1.call-done = bf16[2048,1024]{1,0:T(8,128)(2,1)} async-done(((bf16[256,1024]{1,0:T(8,128)(2,1)}), bf16[2048,1024]{1,0:T(8,128)(2,1)}) %all-gather.2.cloned.1.call-update) | async-done | bytes 4194320 | tf_op jit(solution)/shard_map/all_gather | solution.py:114
  48.6 2.9 %convolution_convert_fusion = bf16[128,1024]{1,0:T(8,128)(2,1)S(1)} fusion(bf16[2048,1024]{1,0:T(8,128)(2,1)} %all-gather.2.cloned.1.call-done, bf16[1,128,2048]{2,1,0:T(8,128)(2,1)S(1)} %copy-done), kind=kOutput, calls=%fused_computation.18 | convolution fusion | flops 537001984 | bytes 4980736 | tf_op jit(solution)/shard_map/dot_general | solution.py:112
  51.5 0.7 copy.131
  52.2 4.6 %all-to-all-start.3 = ((bf16[4,128,256]{2,1,0:T(8,128)(2,1)}), bf16[4,128,256]{2,1,0:T(8,128)(2,1)S(1)}, u32[]{:S(2)}, u32[]{:S(2)}) async-start(bf16[4,128,256]{2,1,0:T(8,128)(2,1)} %bitcast.77), calls=%async_computation.3 | async-start | bytes 524288 | tf_op jit(solution)/shard_map/all_to_all | solution.py:118
  56.8 1.4 fusion.17
  58.6 7.5 %all-to-all-done.3 = bf16[4,128,256]{2,1,0:T(8,128)(2,1)S(1)} async-done(((bf16[4,128,256]{2,1,0:T(8,128)(2,1)}), bf16[4,128,256]{2,1,0:T(8,128)(2,1)S(1)}, u32[]{:S(2)}, u32[]{:S(2)}) %all-to-all-start.3) | async-done | bytes 262176 | tf_op jit(solution)/shard_map/all_to_all | solution.py:118
  66.1 3.5 %all-to-all-start.4 = ((bf16[4,128,512]{2,1,0:T(8,128)(2,1)}), bf16[4,128,512]{2,1,0:T(8,128)(2,1)S(1)}, u32[]{:S(2)}, u32[]{:S(2)}) async-start(bf16[4,128,512]{2,1,0:T(8,128)(2,1)} %bitcast.75), calls=%async_computation.4 | async-start | bytes 1048576 | tf_op jit(solution)/shard_map/all_to_all | solution.py:129
  69.7 1.0 copy.72
  70.7 1.0 convert.4
  71.7 3.1 %multiply_convert_fusion.3 = (bf16[8,64,256]{2,0,1:T(8,128)(2,1)}, bf16[8,64,256]{2,0,1:T(8,128)(2,1)S(1)}, bf16[8,64,256]{2,0,1:T(8,128)(2,1)S(1)}, bf16[8,64,256]{2,0,1:T(8,128)(2,1)S(1)}, bf16[8,64,256]{2,0,1:T(8,128)(2,1)}) fusion(f32[8,64,256]{2,0,1:T(8,128)S(1)} %fusion.20, f32[8,64,256]{2,1,0:T(8,128)S(1)} %convert.4, f32[8,64,256]{2,1,0:T(8,128)} %bitcast.94, ...), kind=kLoop, calls=%fused_computation.37 | loop fusion | flops 1835008 | bytes 3416064 | tf_op jit(solution)/shard_map/convert_element_type | solution.py:41
  74.7 7.9 %all-to-all-done.4 = bf16[4,128,512]{2,1,0:T(8,128)(2,1)S(1)} async-done(((bf16[4,128,512]{2,1,0:T(8,128)(2,1)}), bf16[4,128,512]{2,1,0:T(8,128)(2,1)S(1)}, u32[]{:S(2)}, u32[]{:S(2)}) %all-to-all-start.4) | async-done | bytes 524320 | tf_op jit(solution)/shard_map/all_to_all | solution.py:129
  82.6 2.7 %fusion.26 = f32[8,256,512]{2,1,0:T(8,128)} fusion(bf16[8,64,512]{2,1,0:T(8,128)(2,1)S(1)} %bitcast.90, bf16[8,64,256]{2,0,1:T(8,128)(2,1)S(1)} %get-tuple-element.194), kind=kOutput, calls=%fused_computation.48 | convolution fusion | flops 134217728 | bytes 4980736 | tf_op jit(solution)/shard_map/njd,nje->nde/dot_general | solution.py:62
  85.3 1.5 %broadcast.22.clone = bf16[8,256,512]{2,1,0:T(8,128)(2,1)} broadcast(bf16[]{:T(256)} %constant.115), dimensions={} | broadcast | bytes 2097154 | tf_op jit(solution)/shard_map/broadcast.1
  86.8 16.0 %while.31 = (s32[]{:T(128)}, f32[256,512]{1,0:T(8,128)S(1)}, bf16[8,256,512]{2,1,0:T(8,128)(2,1)}, f32[8,256]{1,0:T(8,128)S(1)}, f32[8,256,512]{2,1,0:T(8,128)}, /*index=5*/s32[]{:T(128)}, s32[]{:T(128)}, s32[]{:T(128)}) while((s32[]{:T(128)}, f32[256,512]{1,0:T(8,128)S(1)}, bf16[8,256,512]{2,1,0:T(8,128)(2,1)}, ...), condition=%wide.region_4.5_spmd.clone, body=%wide.region_3.4_spmd.clone.sunk | while | flops 655364 | bytes 2625656 | solution.py:78
  86.8 0.8 bitcast_dynamic-update-slice_fusion.5
  87.6 1.2 bitcast_add_fusion.5
  88.8 0.8 bitcast_dynamic-update-slice_fusion.5
  89.6 1.2 bitcast_add_fusion.5
  90.8 0.8 bitcast_dynamic-update-slice_fusion.5
  91.6 1.2 bitcast_add_fusion.5
  92.8 0.8 bitcast_dynamic-update-slice_fusion.5
  93.6 1.2 bitcast_add_fusion.5
  94.8 0.8 bitcast_dynamic-update-slice_fusion.5
  95.6 1.2 bitcast_add_fusion.5
  96.8 0.8 bitcast_dynamic-update-slice_fusion.5
  97.7 1.2 bitcast_add_fusion.5
  98.8 0.8 bitcast_dynamic-update-slice_fusion.5
  99.7 1.2 bitcast_add_fusion.5
  100.9 0.8 bitcast_dynamic-update-slice_fusion.5
  101.7 1.2 bitcast_add_fusion.5
  102.9 2.7 %fusion.22 = f32[8,256,512]{2,1,0:T(8,128)} fusion(bf16[8,64,512]{2,1,0:T(8,128)(2,1)S(1)} %bitcast.91, bf16[8,64,256]{2,0,1:T(8,128)(2,1)S(1)} %copy-done.4), kind=kOutput, calls=%fused_computation.44 | convolution fusion | flops 134217728 | bytes 4980736 | tf_op jit(solution)/shard_map/njd,nje->nde/dot_general | solution.py:59
  105.6 1.5 %broadcast.22.clone.1 = bf16[8,256,512]{2,1,0:T(8,128)(2,1)} broadcast(bf16[]{:T(256)} %constant.115), dimensions={} | broadcast | bytes 2097154 | tf_op jit(solution)/shard_map/broadcast.1
  107.1 15.5 %while.30 = (s32[]{:T(128)}, f32[256,512]{1,0:T(8,128)S(1)}, bf16[8,256,512]{2,1,0:T(8,128)(2,1)}, f32[8,256]{1,0:T(8,128)S(1)}, f32[8,256,512]{2,1,0:T(8,128)}, /*index=5*/s32[]{:T(128)}, s32[]{:T(128)}) while((s32[]{:T(128)}, f32[256,512]{1,0:T(8,128)S(1)}, bf16[8,256,512]{2,1,0:T(8,128)(2,1)}, f32[8,256]{1,0:T(8,128)S(1)}, ...), condition=%wide.region_2.3_spmd.clone, body=%wide.region_1.2_spmd.clone.sunk | while | flops 524291 | bytes 2362976 | solution.py:77
  107.1 0.8 bitcast_dynamic-update-slice_fusion.4
  107.9 1.2 bitcast_add_fusion.4
  109.1 0.7 bitcast_dynamic-update-slice_fusion.4
  109.8 1.2 bitcast_add_fusion.4
  111.0 0.8 bitcast_dynamic-update-slice_fusion.4
  111.7 1.2 bitcast_add_fusion.4
  112.9 0.7 bitcast_dynamic-update-slice_fusion.4
  113.7 1.2 bitcast_add_fusion.4
  114.8 0.7 bitcast_dynamic-update-slice_fusion.4
  115.6 1.2 bitcast_add_fusion.4
  116.8 0.7 bitcast_dynamic-update-slice_fusion.4
  117.5 1.2 bitcast_add_fusion.4
  118.7 0.8 bitcast_dynamic-update-slice_fusion.4
  119.5 1.2 bitcast_add_fusion.4
  120.7 0.8 bitcast_dynamic-update-slice_fusion.4
  121.4 1.2 bitcast_add_fusion.4
  122.6 2.2 %fusion = f32[8,64,512]{2,1,0:T(8,128)S(1)} fusion(bf16[8,256,512]{2,1,0:T(8,128)(2,1)} %get-tuple-element.136, bf16[8,64,256]{2,0,1:T(8,128)(2,1)S(1)} %get-tuple-element.195), kind=kOutput, calls=%fused_computation.7 | convolution fusion | flops 134217728 | bytes 3407872 | tf_op jit(solution)/shard_map/tzv,tvg->tzg/dot_general | solution.py:85
  126.0 0.9 pad_maximum_fusion
  126.9 3.5 %all-to-all-start.5 = ((bf16[4,1,128,512]{3,2,1,0:T(8,128)(2,1)}), bf16[4,1,128,512]{3,2,1,0:T(8,128)(2,1)S(1)}, u32[]{:S(2)}, u32[]{:S(2)}) async-start(bf16[4,1,128,512]{3,2,1,0:T(8,128)(2,1)} %pad_maximum_fusion), calls=%async_computation.5 | async-start | bytes 1048576 | tf_op jit(solution)/shard_map/all_to_all | solution.py:19
  130.4 13.2 %all-to-all-done.5 = bf16[4,1,128,512]{3,2,1,0:T(8,128)(2,1)S(1)} async-done(((bf16[4,1,128,512]{3,2,1,0:T(8,128)(2,1)}), bf16[4,1,128,512]{3,2,1,0:T(8,128)(2,1)S(1)}, u32[]{:S(2)}, u32[]{:S(2)}) %all-to-all-start.5) | async-done | bytes 524320 | tf_op jit(solution)/shard_map/all_to_all | solution.py:19
  144.4 1.2 convert_element_type.104
  (54 shorter events, 4.2 us)
Async XLA Ops:
  6.5 8.3 %copy-start = (bf16[1,128,2048]{2,1,0:T(8,128)(2,1)S(1)}, bf16[1,128,2048]{2,1,0:T(8,128)(2,1)}, u32[]{:S(2)}) copy-start(bf16[1,128,2048]{2,1,0:T(8,128)(2,1)} %param.13) | copy-start | bytes 1572868
  6.5 26.7 %copy-start.5 = (bf16[1,128,2048]{2,1,0:T(8,128)(2,1)S(1)}, bf16[1,128,2048]{2,1,0:T(8,128)(2,1)}, u32[]{:S(2)}) copy-start(bf16[1,128,2048]{2,1,0:T(8,128)(2,1)} %param.15) | copy-start | bytes 1572868
  6.5 42.0 %all-gather.2.cloned.1.call-start = ((), (), s32[]{:S(2)}) async-start(), calls=%async_computation.6 | async-start | bytes 4718592 | tf_op jit(solution)/shard_map/all_gather | solution.py:114
  8.5 11.8 %all-to-all-start.2 = ((bf16[4,128,1]{1,2,0:T(2,128)(2,1)}), bf16[4,128,1]{1,2,0:T(2,128)(2,1)S(1)}, u32[]{:S(2)}, u32[]{:S(2)}) async-start(bf16[4,128,1]{1,2,0:T(2,128)(2,1)} %broadcast_in_dim.46), calls=%async_computation.2 | async-start | bytes 4096 | tf_op jit(solution)/shard_map/all_to_all | solution.py:131
  21.0 8.8 %all-to-all-start.1 = ((bf16[4,128,16]{1,2,0:T(8,128)(2,1)}), bf16[4,128,16]{1,2,0:T(8,128)(2,1)S(1)}, u32[]{:S(2)}, u32[]{:S(2)}) async-start(bf16[4,128,16]{1,2,0:T(8,128)(2,1)} %broadcast_in_dim.44), calls=%async_computation.1 | async-start | bytes 32768 | tf_op jit(solution)/shard_map/all_to_all | solution.py:130
  29.8 22.4 %all-to-all-start = ((bf16[4,128,256]{1,2,0:T(8,128)(2,1)}), bf16[4,128,256]{1,2,0:T(8,128)(2,1)S(1)}, u32[]{:S(2)}, u32[]{:S(2)}) async-start(bf16[4,128,256]{1,2,0:T(8,128)(2,1)} %bitcast.1), calls=%async_computation | async-start | bytes 524288 | tf_op jit(solution)/shard_map/all_to_all | solution.py:122
  52.2 13.9 %all-to-all-start.3 = ((bf16[4,128,256]{2,1,0:T(8,128)(2,1)}), bf16[4,128,256]{2,1,0:T(8,128)(2,1)S(1)}, u32[]{:S(2)}, u32[]{:S(2)}) async-start(bf16[4,128,256]{2,1,0:T(8,128)(2,1)} %bitcast.77), calls=%async_computation.3 | async-start | bytes 524288 | tf_op jit(solution)/shard_map/all_to_all | solution.py:118
  58.2 7.9 %copy-start.2 = (f32[512,256]{1,0:T(8,128)}, f32[512,256]{1,0:T(8,128)S(1)}, u32[]{:S(2)}) copy-start(f32[512,256]{1,0:T(8,128)S(1)} %fusion.17) | copy-start | bytes 1572868
  66.1 3.5 %copy-start.3 = (bf16[4,128,256]{2,1,0:T(8,128)(2,1)}, bf16[4,128,256]{2,1,0:T(8,128)(2,1)S(1)}, u32[]{:S(2)}) copy-start(bf16[4,128,256]{2,1,0:T(8,128)(2,1)S(1)} %all-to-all-done.3) | copy-start | bytes 786436
  66.1 16.5 %all-to-all-start.4 = ((bf16[4,128,512]{2,1,0:T(8,128)(2,1)}), bf16[4,128,512]{2,1,0:T(8,128)(2,1)S(1)}, u32[]{:S(2)}, u32[]{:S(2)}) async-start(bf16[4,128,512]{2,1,0:T(8,128)(2,1)} %bitcast.75), calls=%async_computation.4 | async-start | bytes 1048576 | tf_op jit(solution)/shard_map/all_to_all | solution.py:129
  86.8 16.0 %copy-start.4 = (bf16[8,64,256]{2,0,1:T(8,128)(2,1)S(1)}, bf16[8,64,256]{2,0,1:T(8,128)(2,1)}, u32[]{:S(2)}) copy-start(bf16[8,64,256]{2,0,1:T(8,128)(2,1)} %get-tuple-element.197) | copy-start | bytes 786436
  122.6 2.2 %copy-start.6 = (bf16[8,64,256]{2,0,1:T(8,128)(2,1)S(1)}, bf16[8,64,256]{2,0,1:T(8,128)(2,1)}, u32[]{:S(2)}) copy-start(bf16[8,64,256]{2,0,1:T(8,128)(2,1)} %get-tuple-element.193) | copy-start | bytes 786436
  122.6 2.4 %copy-start.1 = (bf16[8,256,512]{2,1,0:T(8,128)(2,1)S(1)}, bf16[8,256,512]{2,1,0:T(8,128)(2,1)}, u32[]{:S(2)}) copy-start(bf16[8,256,512]{2,1,0:T(8,128)(2,1)} %get-tuple-element.135) | copy-start | bytes 6291460
  125.9 4.4 %copy-start.7 = (f32[2048]{0:T(1024)S(1)}, f32[2048]{0:T(1024)}, u32[]{:S(2)}) copy-start(f32[2048]{0:T(1024)} %param.21) | copy-start | bytes 24580
  126.9 16.7 %all-to-all-start.5 = ((bf16[4,1,128,512]{3,2,1,0:T(8,128)(2,1)}), bf16[4,1,128,512]{3,2,1,0:T(8,128)(2,1)S(1)}, u32[]{:S(2)}, u32[]{:S(2)}) async-start(bf16[4,1,128,512]{3,2,1,0:T(8,128)(2,1)} %pad_maximum_fusion), calls=%async_computation.5 | async-start | bytes 1048576 | tf_op jit(solution)/shard_map/all_to_all | solution.py:19
Sparse Core Ops, SparseCore 0:
  9.2 39.2 all-gather.1
